TPU v7x, 32 devices: a whole 2x2x4 slice. The times are simulated.
32 devices in a mesh: sp: 16 (over z, y, core), tp: 2 (over x).
Axes of the slice: x: 2, y: 2, z: 4, core: 2. Of those that a mesh axis runs over, the one named last changes fastest.
Arguments:
- queries: bfloat16 [16384, 1024], P('sp', 'tp'), may hold values from -8 to 8
- keyvals: bfloat16 [16384, 8, 128], P('sp', 'tp'), may hold values from -8 to 8
- head_sink_logit: float32 [16], P('tp'), may hold values from 2 to 7
- doc_ids: int32 [16384], P('sp'), may hold values from 0 to 7, never falling along the last dimension, each value on 1 to 4096 neighbouring positions
- stream_in: bfloat16 [16384, 2048], P(('sp', 'tp')), may hold values from -6 to 6
- out_weight: bfloat16 [1024, 2048], replicated, may hold values from -1.5 to 1.5
- first_gain: float32 [2048], replicated, may hold values from 0.1 to 1.9
- up_weight: bfloat16 [2048, 8192], P('sp', 'tp'), may hold values from -0.125 to 0.125
- down_weight: bfloat16 [8192, 2048], P('tp', 'sp'), may hold values from -0.0625 to 0.0625
- second_gain: float32 [2048], replicated, may hold values from 0.1 to 1.9
Outputs:
- layer_out: bfloat16 [16384, 2048], P(('sp', 'tp'))
Inputs may be any that keep to these rules, and one draw needn't show every extreme that they name: `doc_ids`: document numbers never fall along the sequence.
All inputs are finite; a program needn't handle non-finite values.
Results may differ from a plain program's by a relative error of at most 0.013.
Values may be sent and summed in bfloat16 or wider, within the bound.
A program may use at most 128 MiB of HBM per device.

v0:
```python
import jax
import jax.numpy as jnp
from jax import lax
from jax.sharding import PartitionSpec as P

HEAD_SIZE = 64
WINDOW_REACH = 128
NEG_LARGE = -1e30
NORM_EPS = 1e-05


def padded(block, sides, width):
    for axis, dim in sides:
        count = lax.axis_size(axis)
        forward = [(i, i + 1) for i in range(count - 1)]
        backward = [(target, source) for source, target in forward]
        low = lax.ppermute(
            lax.slice_in_dim(block, block.shape[dim] - width, None, axis=dim), axis, forward
        )
        high = lax.ppermute(lax.slice_in_dim(block, 0, width, axis=dim), axis, backward)
        block = jnp.concatenate([low, block, high], axis=dim)
    return block


def layer_norm(stream, gain_row):
    centre = jnp.mean(stream, axis=-1, keepdims=True)
    shifted = stream - centre
    spread = jnp.mean(shifted * shifted, axis=-1, keepdims=True)
    return shifted * lax.rsqrt(spread + NORM_EPS) * gain_row


def attend(queries, keyvals, head_sink_logit, doc_ids):
    tok_rows = queries.shape[0]
    kv_heads = keyvals.shape[1]
    heads_per_group = queries.shape[1] // (HEAD_SIZE * kv_heads)
    block_list = tok_rows // WINDOW_REACH
    score_scale = HEAD_SIZE ** (-0.5)
    doc_marks = doc_ids.astype(jnp.bfloat16)
    rim_keys, rim_docs = (
        padded(keyvals, (("sp", 0),), WINDOW_REACH),
        padded(doc_marks, (("sp", 0),), WINDOW_REACH),
    )
    padded_rows = rim_keys.reshape(block_list + 2, WINDOW_REACH, kv_heads, 2 * HEAD_SIZE)
    banded = jnp.concatenate([padded_rows[:-2], padded_rows[1:-1], padded_rows[2:]], axis=1)
    doc_ext = rim_docs.reshape(block_list + 2, WINDOW_REACH)
    doc_band = jnp.concatenate([doc_ext[:-2], doc_ext[1:-1], doc_ext[2:]], axis=1)
    offset = lax.axis_index("sp") * tok_rows
    total_rows = tok_rows * lax.axis_size("sp")
    query_pos = offset + jnp.arange(tok_rows, dtype=jnp.int32).reshape(block_list, WINDOW_REACH, 1)
    key_pos = (
        offset
        + (
            jnp.arange(block_list, dtype=jnp.int32)[:, None] * WINDOW_REACH
            + jnp.arange(3 * WINDOW_REACH, dtype=jnp.int32)[None, :]
            - WINDOW_REACH
        )[:, None, :]
    )
    allowed = (
        (jnp.abs(query_pos - key_pos) <= WINDOW_REACH)
        & (key_pos >= 0)
        & (key_pos < total_rows)
        & (doc_marks.reshape(block_list, WINDOW_REACH, 1) == doc_band[:, None, :])
    )
    query_block_list = queries.reshape(
        block_list, WINDOW_REACH, kv_heads, heads_per_group, HEAD_SIZE
    )
    scores = (
        jnp.einsum(
            "nqhgd,nkhd->nhgqk",
            query_block_list,
            banded[..., :HEAD_SIZE],
            preferred_element_type=jnp.float32,
        )
        * score_scale
    )
    scores = jnp.where(allowed[:, None, None], scores, NEG_LARGE)
    sink_col = head_sink_logit.reshape(kv_heads, heads_per_group)[None, :, :, None, None]
    highest = jnp.maximum(jnp.max(scores, axis=-1, keepdims=True), sink_col)
    powers = jnp.exp(scores - highest)
    denominator = jnp.sum(powers, axis=-1, keepdims=True) + jnp.exp(sink_col - highest)
    weights = (powers / denominator).astype(jnp.bfloat16)
    mixed_out = jnp.einsum(
        "nhgqk,nkhd->nqhgd", weights, banded[..., HEAD_SIZE:], preferred_element_type=jnp.float32
    )
    return mixed_out.astype(jnp.bfloat16).reshape(tok_rows, kv_heads * heads_per_group * HEAD_SIZE)


def per_device(
    queries,
    keyvals,
    head_sink_logit,
    doc_ids,
    stream_in,
    out_weight,
    first_gain,
    up_weight,
    down_weight,
    second_gain,
):
    up_whole = lax.all_gather(up_weight, "sp", axis=0, tiled=True)
    down_whole = lax.all_gather(down_weight, "sp", axis=1, tiled=True)
    attended = attend(queries, keyvals, head_sink_logit, doc_ids)
    tp_count = lax.axis_size("tp")
    own_rows = attended.shape[0] // tp_count
    by_peer = attended.reshape(tp_count, own_rows, attended.shape[1])
    projected = jnp.dot(
        lax.all_to_all(by_peer, "tp", split_axis=0, concat_axis=2, tiled=True)[0],
        out_weight,
        preferred_element_type=jnp.float32,
    )[None][0]
    first_stream = layer_norm(stream_in.astype(jnp.float32) + projected, first_gain).astype(
        jnp.bfloat16
    )
    hidden = jnp.dot(
        lax.all_gather(first_stream, "tp", axis=0, tiled=True),
        up_whole,
        preferred_element_type=jnp.float32,
    )
    active = jnp.square(jnp.maximum(hidden, 0.0)).astype(jnp.bfloat16)
    mixed_out = lax.psum_scatter(
        jnp.dot(active, down_whole, preferred_element_type=jnp.float32).astype(jnp.bfloat16),
        "tp",
        scatter_dimension=0,
        tiled=True,
    ).astype(jnp.float32)
    return layer_norm(first_stream.astype(jnp.float32) + mixed_out, second_gain).astype(
        jnp.bfloat16
    )


def solution(mesh):
    return jax.shard_map(
        per_device,
        mesh=mesh,
        in_specs=(
            P("sp", "tp"),
            P("sp", "tp", None),
            P("tp"),
            P("sp"),
            P(("sp", "tp"), None),
            P(),
            P(),
            P("sp", "tp"),
            P("tp", "sp"),
            P(),
        ),
        out_specs=P(("sp", "tp"), None),
        check_vma=False,
    )
```

profile of v0, /device:TPU:0, one launch (start us, length us, event | category | flops | bytes accessed | tf_op | source)
XLA Modules:
  0.0 477.8 jit_solution(12057201046544516895)
XLA Ops:
  6.5 0.8 convert_element_type.34
  7.3 2.4 collective-permute-start.2
  9.7 1.3 collective-permute-start.3
  11.0 1.4 copy.26
  12.4 5.8 %collective-permute-start = (bf16[128,4,128]{2,0,1:T(8,128)(2,1)S(1)}, bf16[128,4,128]{2,0,1:T(8,128)(2,1)}, u32[]{:S(2)}, u32[]{:S(2)}) collective-permute-start(bf16[128,4,128]{2,0,1:T(8,128)(2,1)S(1)} %get-tuple-element.7), channel_id=1, source_target_pairs={{0,2},{2,4},{4,6},{6,8},{8,10},{10,12},{12,14},{14,16},{16,18},{18... | collective-permute-start | bytes 393224 | tf_op jit(solution)/shard_map/ppermute | solution.py:17
  18.2 1.3 collective-permute-start.1
  19.5 0.7 convert_bitcast_fusion
  20.4 2.3 copy.32
  22.6 2.1 reshape.167
  24.8 2.3 fusion.9
  27.1 1.3 pad_maximum_fusion.2
  29.7 1.8 pad_maximum_fusion
  31.6 2.5 fusion.1
  34.3 3.4 fusion
  37.8 3.6 fusion.11
  41.4 0.7 copy.37
  42.8 17.2 %all_to_all.15 = bf16[2,512,512]{1,2,0:T(8,128)(2,1)S(1)} all-to-all(bf16[2,512,512]{1,2,0:T(8,128)(2,1)S(1)} %copy.38), channel_id=1, replica_groups=mesh['sp'=16,'tp'=2] {'tp'}, dimensions={0} | all-to-all | bytes 2097152 | tf_op jit(solution)/shard_map/all_to_all | solution.py:107
  60.0 4.2 fusion.20
  64.8 1.4 copy-done
  66.1 1.9 multiply_convert_fusion.2
  68.1 0.7 all-gather.6.cloned.1.call-update
  68.9 0.7 all-gather.8.cloned.1.call-update
  69.6 56.9 %all-gather.4.cloned.1.call-done = bf16[1024,2048]{1,0:T(8,128)(2,1)} async-done(((bf16[512,2048]{1,0:T(8,128)(2,1)}), bf16[1024,2048]{1,0:T(8,128)(2,1)}) %all-gather.4.cloned.1.call-update) | async-done | bytes 4194320 | tf_op jit(solution)/shard_map/all_gather | solution.py:115
  126.5 128.6 %all-gather.6.cloned.1.call-done = bf16[2048,4096]{1,0:T(8,128)(2,1)} async-done(((bf16[128,4096]{1,0:T(8,128)(2,1)}), bf16[2048,4096]{1,0:T(8,128)(2,1)}) %all-gather.6.cloned.1.call-update) | async-done | bytes 16777232 | tf_op jit(solution)/shard_map/all_gather | solution.py:100
  255.1 22.9 %fusion.44 = bf16[1024,4096]{1,0:T(8,128)(2,1)} fusion(bf16[2048,4096]{1,0:T(8,128)(2,1)} %all-gather.6.cloned.1.call-done, bf16[1024,2048]{1,0:T(8,128)(2,1)} %all-gather.4.cloned.1.call-done), kind=kOutput, calls=%bitcast_fusion.1.clone.1 | convolution fusion | flops 17192452096 | bytes 29360128 | tf_op jit(solution)/shard_map/dot_general | solution.py:114
  278.0 107.4 %all-gather.8.cloned.1.call-done = bf16[4096,2048]{1,0:T(8,128)(2,1)} async-done(((bf16[4096,128]{1,0:T(8,128)(2,1)}), bf16[4096,2048]{1,0:T(8,128)(2,1)}) %all-gather.8.cloned.1.call-update) | async-done | bytes 16777232 | tf_op jit(solution)/shard_map/all_gather | solution.py:101
  385.4 23.7 %convolution_convert_fusion = bf16[1024,2048]{1,0:T(8,128)(2,1)} fusion(bf16[4096,2048]{1,0:T(8,128)(2,1)} %all-gather.8.cloned.1.call-done, bf16[1024,4096]{1,0:T(8,128)(2,1)} %fusion.44), kind=kOutput, calls=%fused_computation.15 | convolution fusion | flops 17181966336 | bytes 29360128 | tf_op jit(solution)/shard_map/dot_general | solution.py:121
  409.1 52.7 %reduce-scatter.2.cloned.1.call-done = bf16[512,2048]{1,0:T(8,128)(2,1)} async-done(((bf16[1024,2048]{1,0:T(8,128)(2,1)}), bf16[512,2048]{1,0:T(8,128)(2,1)}) %reduce-scatter.2.cloned.1.call-update) | async-done | bytes 2097168 | tf_op jit(solution)/shard_map/reduce_scatter | solution.py:120
  461.8 3.9 fusion.4
  465.8 0.7 copy-done.2
  466.5 1.2 multiply_reduce_fusion
  467.8 3.5 multiply_convert_fusion.1
  (50 shorter events, 3.3 us)
Async XLA Ops:
  6.5 16.1 %copy-start.7 = (bf16[1024,512]{1,0:T(8,128)(2,1)S(1)}, bf16[1024,512]{1,0:T(8,128)(2,1)}, u32[]{:S(2)}) copy-start(bf16[1024,512]{1,0:T(8,128)(2,1)} %param.10) | copy-start | bytes 3145732
  6.5 18.2 %copy-start.10 = (f32[8]{0:T(128)S(1)}, f32[8]{0:T(128)}, u32[]{:S(2)}) copy-start(f32[8]{0:T(128)} %param.12) | copy-start | bytes 100
  6.5 119.9 %all-gather.4.cloned.1.call-start = ((), (), s32[]{:S(2)}) async-start(), calls=%async_computation.2 | async-start | bytes 6291456 | tf_op jit(solution)/shard_map/all_gather | solution.py:115
  7.3 17.5 %collective-permute-start.2 = (bf16[128]{0:T(256)(128)(2,1)S(1)}, bf16[128]{0:T(256)(128)(2,1)S(1)}, u32[]{:S(2)}, u32[]{:S(2)}) collective-permute-start(bf16[128]{0:T(256)(128)(2,1)S(1)} %get-tuple-element.11), channel_id=1, source_target_pairs={{0,2},{2,4},{4,6},{6,8},{8,10},{10,12},{12,14},{14,16},{16,18},{18... | collective-permute-start | bytes 776 | tf_op jit(solution)/shard_map/ppermute | solution.py:17
  9.7 15.1 %collective-permute-start.3 = (bf16[128]{0:T(256)(128)(2,1)S(1)}, bf16[128]{0:T(256)(128)(2,1)S(1)}, u32[]{:S(2)}, u32[]{:S(2)}) collective-permute-start(bf16[128]{0:T(256)(128)(2,1)S(1)} %get-tuple-element.12), channel_id=1, source_target_pairs={{2,0},{4,2},{6,4},{8,6},{10,8},{12,10},{14,12},{16,14},{18,16},{20... | collective-permute-start | bytes 776 | tf_op jit(solution)/shard_map/ppermute | solution.py:20
  12.4 14.7 %collective-permute-start = (bf16[128,4,128]{2,0,1:T(8,128)(2,1)S(1)}, bf16[128,4,128]{2,0,1:T(8,128)(2,1)}, u32[]{:S(2)}, u32[]{:S(2)}) collective-permute-start(bf16[128,4,128]{2,0,1:T(8,128)(2,1)S(1)} %get-tuple-element.7), channel_id=1, source_target_pairs={{0,2},{2,4},{4,6},{6,8},{8,10},{10,12},{12,14},{14,16},{16,18},{18... | collective-permute-start | bytes 393224 | tf_op jit(solution)/shard_map/ppermute | solution.py:17
  18.2 8.9 %collective-permute-start.1 = (bf16[128,4,128]{2,0,1:T(8,128)(2,1)S(1)}, bf16[128,4,128]{2,0,1:T(8,128)(2,1)}, u32[]{:S(2)}, u32[]{:S(2)}) collective-permute-start(bf16[128,4,128]{2,0,1:T(8,128)(2,1)S(1)} %get-tuple-element.8), channel_id=1, source_target_pairs={{2,0},{4,2},{6,4},{8,6},{10,8},{12,10},{14,12},{16,14},{18,16},{20... | collective-permute-start | bytes 393224 | tf_op jit(solution)/shard_map/ppermute | solution.py:20
  29.7 1.9 copy-start.6
  31.6 2.5 copy-start.4
  34.3 3.6 copy-start.5
  42.6 17.4 %copy-start.3 = (bf16[1024,2048]{1,0:T(8,128)(2,1)S(1)}, bf16[1024,2048]{1,0:T(8,128)(2,1)}, u32[]{:S(2)}) copy-start(bf16[1024,2048]{1,0:T(8,128)(2,1)} %param.15) | copy-start | bytes 12582916
  64.2 1.9 copy-start
  64.2 1.9 copy-start.8
  68.1 187.0 %all-gather.6.cloned.1.call-start = ((), (), s32[]{:S(2)}) async-start(), calls=%async_computation.3 | async-start | bytes 17825792 | tf_op jit(solution)/shard_map/all_gather | solution.py:100
  68.8 316.5 %all-gather.8.cloned.1.call-start = ((), (), s32[]{:S(2)}) async-start(), calls=%async_computation.4 | async-start | bytes 17825792 | tf_op jit(solution)/shard_map/all_gather | solution.py:101
  69.6 392.2 %reduce-scatter.2.cloned.1.call-start = ((), (), s32[]{:S(2)}) async-start(), calls=%async_computation.5 | async-start | bytes 6291456 | tf_op jit(solution)/shard_map/reduce_scatter | solution.py:120
  461.8 4.0 copy-start.1
  461.8 4.7 copy-start.2
  465.7 2.0 copy-start.9
Sparse Core Ops, SparseCore 0:
  68.2 58.2 all-gather.3
  128.6 126.4 all-gather.5
  257.3 128.0 all-gather.7
  409.2 52.5 reduce-scatter.1
where the time goes:
time: 478 us
  waiting for transfers between devices  347 us (73%)
  matrix products  56.9 us (12%)
  other arithmetic  21.8 us (5%)
  blocking collectives  17.2 us (4%)
  between operations  13.4 us (3%)
  starting transfers between devices  10.9 us (2%)
  local copies, waits for them, and re-layouts  10.6 us (2%)
    all_gather x1, waiting for transfers between devices, per_device(): up_whole = lax.all_gather(up_weight, 'sp', axis=0, tiled=True)  129 us
    all_gather x1, waiting for transfers between devices, per_device(): down_whole = lax.all_gather(down_weight, 'sp', axis=1, tiled=True)  107 us
    all_gather x1, waiting for transfers between devices, per_device(): lax.all_gather(first_stream, 'tp', axis=0, tiled=True)  56.9 us
    reduce_scatter x1, waiting for transfers between devices, per_device(): lax.psum_scatter(jnp.dot(active, down_whole, preferred_element_type=jnp.f...  52.7 us
    dot_general x1, matrix products, per_device(): jnp.dot(active, down_whole, preferred_element_type=jnp.float32)  23.7 us
    dot_general x1, matrix products, per_device(): jnp.dot(lax.all_gather(first_stream, 'tp', axis=0, tiled=True), up_whole,...  22.9 us
    all_to_all x1, blocking collectives, per_device(): lax.all_to_all(by_peer, 'tp', split_axis=0, concat_axis=2, tiled=True)[0]  17.2 us
  transfers between devices with their start and end apart: 8, of which 4 were waited for; matrix products, arithmetic and copies ran while one was open for 7% of the time, Pallas kernels for 0%

commit v1 on v0

--- a/solution.py
+++ b/solution.py
@@ -98,7 +98,8 @@
     second_gain,
 ):
     up_whole = lax.all_gather(up_weight, "sp", axis=0, tiled=True)
-    down_whole = lax.all_gather(down_weight, "sp", axis=1, tiled=True)
+    terms_view = lambda state, device_axis: jnp.concatenate(lax.all_gather(state, device_axis), 1)
+    down_whole = terms_view(down_weight, "sp")
     attended = attend(queries, keyvals, head_sink_logit, doc_ids)
     tp_count = lax.axis_size("tp")
     own_rows = attended.shape[0] // tp_count

time: 478 us -> 439 us (0.918)
  waiting for transfers between devices: 347 us -> 286 us
  local copies, waits for them, and re-layouts: 10.6 us -> 32.3 us
    all_gather x1, waiting for transfers between devices: 107 us -> 68 us  [per_device(): lax.all_gather(state, device_axis)]
    all_gather x1, waiting for transfers between devices: 56.9 us -> 35.3 us  [per_device(): lax.all_gather(first_stream, 'tp', axis=0, tiled=True)]
    reshape x0 -> x1, local copies, waits for them, and re-layouts: none -> 21.2 us  [per_device(): jnp.concatenate(lax.all_gather(state, device_axis), 1)]
  transfers between devices with their start and end apart: 8 -> 8, of which waited for: 4 -> 4; matrix products, arithmetic and copies ran while one was open for 7% -> 13% of each run, Pallas kernels for 0% -> 0%
where the time goes in v1:
time: 439 us; the launch traced here: 438 us
  waiting for transfers between devices  286 us (65%)
  matrix products  54.7 us (12%)
  local copies, waits for them, and re-layouts  32.3 us (7%)
  other arithmetic  23.8 us (5%)
  blocking collectives  17.2 us (4%)
  between operations  13.4 us (3%)
  starting transfers between devices  10.9 us (2%)
    all_gather x1, waiting for transfers between devices, per_device(): up_whole = lax.all_gather(up_weight, 'sp', axis=0, tiled=True)  129 us
    all_gather x1, waiting for transfers between devices, per_device(): lax.all_gather(state, device_axis)  68 us
    reduce_scatter x1, waiting for transfers between devices, per_device(): lax.psum_scatter(jnp.dot(active, down_whole, preferred_element_type=jnp.f...  52.7 us
    all_gather x1, waiting for transfers between devices, per_device(): lax.all_gather(first_stream, 'tp', axis=0, tiled=True)  35.3 us
    dot_general x1, matrix products, per_device(): jnp.dot(lax.all_gather(first_stream, 'tp', axis=0, tiled=True), up_whole,...  23 us
    dot_general x1, matrix products, per_device(): jnp.dot(active, down_whole, preferred_element_type=jnp.float32)  21.4 us
    reshape x1, local copies, waits for them, and re-layouts, per_device(): jnp.concatenate(lax.all_gather(state, device_axis), 1)  21.2 us
    all_to_all x1, blocking collectives, per_device(): lax.all_to_all(by_peer, 'tp', split_axis=0, concat_axis=2, tiled=True)[0]  17.2 us
  transfers between devices with their start and end apart: 8, of which 4 were waited for; matrix products, arithmetic and copies ran while one was open for 13% of the time, Pallas kernels for 0%

profile of v1, /device:TPU:0, one launch (start us, length us, event | category | flops | bytes accessed | tf_op | source)
XLA Modules:
  0.0 438.3 jit_solution(6287170292320835710)
XLA Ops:
  6.5 0.7 all-gather.9.cloned.1.call-update
  7.3 0.7 convert_element_type.34
  8.0 2.4 collective-permute-start.2
  10.4 1.3 collective-permute-start.3
  11.7 1.4 copy.40
  13.1 0.8 fusion.18
  13.8 5.8 %collective-permute-start = (bf16[128,4,128]{2,0,1:T(8,128)(2,1)}, bf16[128,4,128]{2,0,1:T(8,128)(2,1)}, u32[]{:S(2)}, u32[]{:S(2)}) collective-permute-start(bf16[128,4,128]{2,0,1:T(8,128)(2,1)} %get-tuple-element.7), channel_id=1, source_target_pairs={{0,2},{2,4},{4,6},{6,8},{8,10},{10,12},{12,14},{14,16},{16,18},{18... | collective-permute-start | bytes 393224 | tf_op jit(solution)/shard_map/ppermute | solution.py:17
  19.6 1.3 collective-permute-start.1
  21.5 0.7 convert_bitcast_fusion
  23.0 1.3 copy.46
  24.3 2.1 reshape.176
  27.1 3.1 fusion.9
  30.2 1.3 pad_maximum_fusion.2
  32.8 1.8 pad_maximum_fusion
  34.7 2.5 fusion.1
  37.4 3.4 fusion
  40.9 3.6 fusion.11
  44.5 0.7 copy.51
  45.9 17.2 %all_to_all.15 = bf16[2,512,512]{1,2,0:T(8,128)(2,1)S(1)} all-to-all(bf16[2,512,512]{1,2,0:T(8,128)(2,1)S(1)} %copy.52), channel_id=1, replica_groups=mesh['sp'=16,'tp'=2] {'tp'}, dimensions={0} | all-to-all | bytes 2097152 | tf_op jit(solution)/shard_map/all_to_all | solution.py:108
  63.0 4.2 fusion.20
  67.8 1.5 copy-done
  69.3 1.9 multiply_convert_fusion.2
  72.1 68.0 %all-gather.9.cloned.1.call-done = bf16[65536,128]{1,0:T(8,128)(2,1)} async-done(((bf16[4096,128]{1,0:T(8,128)(2,1)}), bf16[65536,128]{1,0:T(8,128)(2,1)}) %all-gather.9.cloned.1.call-update) | async-done | bytes 16777232 | tf_op jit(solution)/shard_map/all_gather | solution.py:101
  140.0 21.2 %copy.53 = bf16[4096,16,128]{0,2,1:T(8,128)(2,1)} copy(bf16[4096,16,128]{2,0,1:T(8,128)(2,1)} %bitcast.78) | data formatting | bytes 33554432 | tf_op jit(solution)/shard_map/reshape | solution.py:101
  161.2 35.3 %all-gather.5.cloned.1.call-done = bf16[1024,2048]{1,0:T(8,128)(2,1)} async-done(((bf16[512,2048]{1,0:T(8,128)(2,1)}), bf16[1024,2048]{1,0:T(8,128)(2,1)}) %all-gather.5.cloned.1.call-update) | async-done | bytes 4194320 | tf_op jit(solution)/shard_map/all_gather | solution.py:116
  196.5 128.6 %all-gather.7.cloned.1.call-done = bf16[2048,4096]{1,0:T(8,128)(2,1)} async-done(((bf16[128,4096]{1,0:T(8,128)(2,1)}), bf16[2048,4096]{1,0:T(8,128)(2,1)}) %all-gather.7.cloned.1.call-update) | async-done | bytes 16777232 | tf_op jit(solution)/shard_map/all_gather | solution.py:100
  325.1 23.0 %fusion.44 = bf16[1024,4096]{1,0:T(8,128)(2,1)} fusion(bf16[2048,4096]{1,0:T(8,128)(2,1)} %all-gather.7.cloned.1.call-done, bf16[1024,2048]{1,0:T(8,128)(2,1)} %all-gather.5.cloned.1.call-done), kind=kOutput, calls=%bitcast_fusion.1.clone.1 | convolution fusion | flops 17192452096 | bytes 29360128 | tf_op jit(solution)/shard_map/dot_general | solution.py:115
  348.2 21.4 %convolution_convert_fusion = bf16[1024,2048]{1,0:T(8,128)(2,1)} fusion(bf16[4096,2048]{0,1:T(8,128)(2,1)S(1)} %bitcast.79, bf16[1024,4096]{1,0:T(8,128)(2,1)} %fusion.44), kind=kOutput, calls=%fused_computation.15 | convolution fusion | flops 17181966336 | bytes 29360128 | tf_op jit(solution)/shard_map/dot_general | solution.py:122
  369.5 52.7 %reduce-scatter.2.cloned.1.call-done = bf16[512,2048]{1,0:T(8,128)(2,1)} async-done(((bf16[1024,2048]{1,0:T(8,128)(2,1)}), bf16[512,2048]{1,0:T(8,128)(2,1)}) %reduce-scatter.2.cloned.1.call-update) | async-done | bytes 2097168 | tf_op jit(solution)/shard_map/reduce_scatter | solution.py:121
  422.2 3.9 fusion.4
  426.9 1.2 multiply_reduce_fusion
  428.2 3.5 multiply_convert_fusion.1
  (57 shorter events, 6.4 us)
Async XLA Ops:
  6.5 16.4 %copy-start.5 = (bf16[1024,4,128]{2,1,0:T(4,128)(2,1)S(1)}, bf16[1024,4,128]{2,1,0:T(4,128)(2,1)}, u32[]{:S(2)}) copy-start(bf16[1024,4,128]{2,1,0:T(4,128)(2,1)} %param.11) | copy-start | bytes 3145732
  6.5 17.8 %copy-start.9 = (bf16[1024,512]{1,0:T(8,128)(2,1)S(1)}, bf16[1024,512]{1,0:T(8,128)(2,1)}, u32[]{:S(2)}) copy-start(bf16[1024,512]{1,0:T(8,128)(2,1)} %param.10) | copy-start | bytes 3145732
  6.5 133.5 %all-gather.9.cloned.1.call-start = ((), (), s32[]{:S(2)}) async-start(), calls=%async_computation.5 | async-start | bytes 17825792 | tf_op jit(solution)/shard_map/all_gather | solution.py:101
  7.3 19.1 %copy-start.13 = (f32[8]{0:T(128)S(1)}, f32[8]{0:T(128)}, u32[]{:S(2)}) copy-start(f32[8]{0:T(128)} %param.12) | copy-start | bytes 100
  7.3 189.2 %all-gather.5.cloned.1.call-start = ((), (), s32[]{:S(2)}) async-start(), calls=%async_computation.2 | async-start | bytes 6291456 | tf_op jit(solution)/shard_map/all_gather | solution.py:116
  8.0 19.0 %collective-permute-start.2 = (bf16[128]{0:T(256)(128)(2,1)S(1)}, bf16[128]{0:T(256)(128)(2,1)S(1)}, u32[]{:S(2)}, u32[]{:S(2)}) collective-permute-start(bf16[128]{0:T(256)(128)(2,1)S(1)} %get-tuple-element.11), channel_id=1, source_target_pairs={{0,2},{2,4},{4,6},{6,8},{8,10},{10,12},{12,14},{14,16},{16,18},{18... | collective-permute-start | bytes 776 | tf_op jit(solution)/shard_map/ppermute | solution.py:17
  10.4 16.6 %collective-permute-start.3 = (bf16[128]{0:T(256)(128)(2,1)S(1)}, bf16[128]{0:T(256)(128)(2,1)S(1)}, u32[]{:S(2)}, u32[]{:S(2)}) collective-permute-start(bf16[128]{0:T(256)(128)(2,1)S(1)} %get-tuple-element.12), channel_id=1, source_target_pairs={{2,0},{4,2},{6,4},{8,6},{10,8},{12,10},{14,12},{16,14},{18,16},{20... | collective-permute-start | bytes 776 | tf_op jit(solution)/shard_map/ppermute | solution.py:20
  13.8 16.4 %collective-permute-start = (bf16[128,4,128]{2,0,1:T(8,128)(2,1)}, bf16[128,4,128]{2,0,1:T(8,128)(2,1)}, u32[]{:S(2)}, u32[]{:S(2)}) collective-permute-start(bf16[128,4,128]{2,0,1:T(8,128)(2,1)} %get-tuple-element.7), channel_id=1, source_target_pairs={{0,2},{2,4},{4,6},{6,8},{8,10},{10,12},{12,14},{14,16},{16,18},{18... | collective-permute-start | bytes 393224 | tf_op jit(solution)/shard_map/ppermute | solution.py:17
  19.6 10.6 %collective-permute-start.1 = (bf16[128,4,128]{2,0,1:T(8,128)(2,1)}, bf16[128,4,128]{2,0,1:T(8,128)(2,1)}, u32[]{:S(2)}, u32[]{:S(2)}) collective-permute-start(bf16[128,4,128]{2,0,1:T(8,128)(2,1)} %get-tuple-element.8), channel_id=1, source_target_pairs={{2,0},{4,2},{6,4},{8,6},{10,8},{12,10},{14,12},{16,14},{18,16},{20... | collective-permute-start | bytes 393224 | tf_op jit(solution)/shard_map/ppermute | solution.py:20
  32.8 1.9 copy-start.8
  34.7 2.5 copy-start.6
  34.7 2.6 copy-start.11
  37.4 3.6 copy-start.7
  45.7 17.4 %copy-start.4 = (bf16[1024,2048]{1,0:T(8,128)(2,1)S(1)}, bf16[1024,2048]{1,0:T(8,128)(2,1)}, u32[]{:S(2)}) copy-start(bf16[1024,2048]{1,0:T(8,128)(2,1)} %param.15) | copy-start | bytes 12582916
  67.3 2.0 copy-start
  67.3 2.0 copy-start.10
  71.3 253.9 %all-gather.7.cloned.1.call-start = ((), (), s32[]{:S(2)}) async-start(), calls=%async_computation.3 | async-start | bytes 17825792 | tf_op jit(solution)/shard_map/all_gather | solution.py:100
  72.0 350.2 %reduce-scatter.2.cloned.1.call-start = ((), (), s32[]{:S(2)}) async-start(), calls=%async_computation.4 | async-start | bytes 6291456 | tf_op jit(solution)/shard_map/reduce_scatter | solution.py:121
  325.1 23.0 %copy-start.3 = (bf16[4096,16,128]{0,2,1:T(8,128)(2,1)S(1)}, bf16[4096,16,128]{0,2,1:T(8,128)(2,1)}, u32[]{:S(2)}) copy-start(bf16[4096,16,128]{0,2,1:T(8,128)(2,1)} %copy.53) | copy-start | bytes 50331652
  422.2 4.0 copy-start.1
  422.2 4.7 %copy-start.2 = (bf16[512,2048]{1,0:T(8,128)(2,1)S(1)}, bf16[512,2048]{1,0:T(8,128)(2,1)}, u32[]{:S(2)}) copy-start(bf16[512,2048]{1,0:T(8,128)(2,1)} %reduce-scatter.2.cloned.1.call-done) | copy-start | bytes 6291460
  426.2 2.0 copy-start.12
Sparse Core Ops, SparseCore 0:
  9.5 130.4 all-gather.8
  141.6 54.8 all-gather.4
  198.7 126.4 all-gather.6
  369.7 52.5 reduce-scatter.1
